TPU v7x, 32 devices: a whole 2x2x4 slice. The times are simulated.
32 devices in a mesh: sp: 8 (over z, core), tp: 4 (over y, x).
Axes of the slice: x: 2, y: 2, z: 4, core: 2. Of those that a mesh axis runs over, the one named last changes fastest.
Arguments:
- cotangent: bfloat16 [1024, 2048], P('sp', 'tp'), may hold values from -3 to 3
- moe_input: bfloat16 [1024, 2048], P('sp', 'tp'), may hold values from -6 to 6
- expert_ids: int32 [1024, 2], P('sp'), may hold values from 0 to 7, all different within a row; in each aligned block of 128 rows (0 to 127, 128 to 255, ...) at most 48 rows name the same one
- group_gate: float32 [1024], P('sp'), may hold values from 0.3 to 1
- expert_gate: float32 [1024, 2], P('sp'), may hold values from 0.1 to 0.9
- weight_gate: bfloat16 [8, 2048, 512], P('sp', None, 'tp'), may hold values from -0.125 to 0.125
- weight_up: bfloat16 [8, 2048, 512], P('sp', None, 'tp'), may hold values from -0.125 to 0.125
- weight_down: bfloat16 [8, 512, 2048], P('sp', 'tp'), may hold values from -0.25 to 0.25
- out_weight: bfloat16 [2048, 1024], P(None, 'tp'), may hold values from -0.1875 to 0.1875
- mixer_out: bfloat16 [1024, 1024], P('sp', 'tp'), may hold values from -6 to 6
- queries: bfloat16 [1024, 512], P('sp', 'tp'), may hold values from -6 to 6
- key_vectors: bfloat16 [1024, 512], P('sp', 'tp'), may hold values from -6 to 6
- values: bfloat16 [1024, 1024], P('sp', 'tp'), may hold values from -6 to 6
- log_decay: float32 [1024, 512], P('sp', 'tp'), may hold values from -0.9 to 0
Outputs:
- grad_gate: bfloat16 [8, 2048, 512], P('sp', None, 'tp')
- grad_up: bfloat16 [8, 2048, 512], P('sp', None, 'tp')
- grad_down: bfloat16 [8, 512, 2048], P('sp', 'tp')
- proj_grad: float32 [2048, 1024], P('sp', 'tp')
- grad_queries: bfloat16 [1024, 512], P('sp', 'tp')
- grad_keys: bfloat16 [1024, 512], P('sp', 'tp')
- grad_values: bfloat16 [1024, 1024], P('sp', 'tp')
- grad_decay: float32 [1024, 512], P('sp', 'tp')
Inputs may be any that keep to these rules, and one draw needn't show every extreme that they name: `expert_ids`: in the rows of one index of sp no expert is named by more than 48 rows, a bound that some block reaches.
All inputs are finite; a program needn't handle non-finite values.
Results may differ from a plain program's by a relative error of at most 0.013.
Values may be sent and summed in bfloat16 or wider, within the bound.
A program may use at most 128 MiB of HBM per device.

v0:
```python
import jax
import jax.numpy as jnp
from jax import lax
from jax.sharding import PartitionSpec as P

DK = 128
DV = 256
TOK = 128
BLK = 64


HIGHEST = lax.Precision.HIGHEST


def carried_in(part, axis, combine, identity, reverse):
    count = lax.axis_size(axis)
    place = lax.axis_index(axis)
    ahead = count - 1 - place if reverse else place
    gathered = jax.tree.map(lambda a: lax.all_gather(a, axis), part)
    state = jax.tree.map(lambda a, e: jnp.zeros_like(a) + jnp.asarray(e, a.dtype), part, identity)

    def one(lap, state):
        source = count - 1 - lap if reverse else lap
        return combine(
            state, jax.tree.map(lambda a: lax.dynamic_index_in_dim(a, source, 0, False), gathered)
        )

    return lax.fori_loop(0, ahead, one, state)


def local_forward(query_heads, key_heads, value_heads, decay_heads, state_in):
    head_count, row_count = (query_heads.shape[0], query_heads.shape[1])
    block_count = row_count // BLK
    causal = jnp.tril(jnp.ones((BLK, BLK), dtype=bool))
    causal_wide = causal[None, :, :, None]

    def blocked(tensor):
        return jnp.moveaxis(tensor.reshape(head_count, block_count, BLK, tensor.shape[-1]), 1, 0)

    def block_step(running, pieces):
        query_blk, key_blk, value_blk, decay_blk = pieces
        cumulative = jnp.cumsum(decay_blk, axis=1)
        block_end = cumulative[:, -1:, :]
        query_scaled = query_blk * DK ** (-0.5)
        query_dec = query_scaled * jnp.exp(cumulative)
        key_end = key_blk * jnp.exp(block_end - cumulative)
        spread = jnp.where(causal_wide, cumulative[:, :, None, :] - cumulative[:, None, :, :], 0.0)
        pair_decay = jnp.where(causal_wide, jnp.exp(spread), 0.0)
        scores = jnp.einsum(
            "hcd,hsd,hcsd->hcs", query_scaled, key_blk, pair_decay, precision=HIGHEST
        )
        outputs = jnp.einsum("hcs,hsv->hcv", scores, value_blk, precision=HIGHEST)
        outputs = outputs + jnp.einsum("hcd,hdv->hcv", query_dec, running, precision=HIGHEST)
        running = jnp.exp(block_end[:, 0, :])[:, :, None] * running + jnp.einsum(
            "hcd,hcv->hdv", key_end, value_blk, precision=HIGHEST
        )
        return (running, outputs)

    state_out, outputs = lax.scan(
        block_step,
        state_in,
        (blocked(query_heads), blocked(key_heads), blocked(value_heads), blocked(decay_heads)),
    )
    return (jnp.moveaxis(outputs, 0, 1).reshape(head_count, row_count, -1), state_out)


def heads_first(tensor, width_in):
    return tensor.astype(jnp.float32).reshape(tensor.shape[0], -1, width_in).transpose(1, 0, 2)


def tokens_first(tensor):
    return tensor.transpose(1, 0, 2).reshape(tensor.shape[1], -1)


def expert_back(routed, inputs, w_gate, w_up, w_down):
    gate_pre = jnp.dot(inputs, w_gate, preferred_element_type=jnp.float32)
    up_pre = jnp.dot(inputs, w_up, preferred_element_type=jnp.float32)
    sigmoid_g = jax.nn.sigmoid(gate_pre)
    active = gate_pre * sigmoid_g
    hidden = (active * up_pre).astype(jnp.bfloat16)
    back_grad = lax.dot_general(
        routed, w_down, (((1,), (1,)), ((), ())), preferred_element_type=jnp.float32
    )
    d_up = (back_grad * active).astype(jnp.bfloat16)
    d_gate = (back_grad * up_pre * sigmoid_g * (1.0 + gate_pre * (1.0 - sigmoid_g))).astype(
        jnp.bfloat16
    )
    contract = (((0,), (0,)), ((), ()))
    grad_down = lax.dot_general(
        hidden, routed, contract, preferred_element_type=jnp.float32
    ).astype(jnp.bfloat16)
    grad_gate = lax.dot_general(
        inputs, d_gate, contract, preferred_element_type=jnp.float32
    ).astype(jnp.bfloat16)
    grad_up = lax.dot_general(inputs, d_up, contract, preferred_element_type=jnp.float32).astype(
        jnp.bfloat16
    )
    return (grad_gate, grad_up, grad_down, d_gate, d_up)


def join_states(earlier, later):
    return (earlier[0] * later[0], later[0][:, :, None] * earlier[1] + later[1])


def shards(
    cotangent,
    moe_input,
    expert_ids,
    group_gate,
    expert_gate,
    weight_gate,
    weight_up,
    weight_down,
    out_weight,
    mixer_out,
    queries,
    key_vectors,
    values,
    log_decay,
):
    tokens = expert_ids.shape[0]
    experts = lax.axis_size("sp")
    capacity = max(2, 3 * TOK // experts)
    flat_ids = expert_ids.reshape(-1)
    onehot = (flat_ids[:, None] == jnp.arange(experts, dtype=jnp.int32)[None, :]).astype(jnp.int32)
    before = jnp.cumsum(onehot, axis=0) - onehot
    position = jnp.sum(before * onehot, axis=1)
    slot_index = flat_ids * capacity + position
    slot_match = slot_index[:, None] == jnp.arange(experts * capacity, dtype=jnp.int32)[None, :]
    route_weight = (group_gate[:, None] * expert_gate).reshape(-1)
    slot_weight = jnp.sum(jnp.where(slot_match, route_weight[:, None], 0.0), axis=0)
    picker = jnp.any(slot_match.reshape(tokens, 2, -1), axis=1).astype(jnp.bfloat16)
    contract = (((0,), (0,)), ((), ()))
    pulled_grad = lax.dot_general(picker, cotangent, contract, preferred_element_type=jnp.float32)
    pulled_in = lax.dot_general(
        picker, moe_input, contract, preferred_element_type=jnp.float32
    ).astype(jnp.bfloat16)
    routed = (slot_weight[:, None] * pulled_grad).astype(jnp.bfloat16)
    routed, rows_in = (
        routed.reshape(experts, capacity, -1),
        pulled_in.reshape(experts, capacity, -1),
    )
    routed, rows_in = (
        lax.all_to_all(routed, "sp", split_axis=0, concat_axis=0, tiled=True),
        lax.all_to_all(rows_in, "sp", split_axis=0, concat_axis=0, tiled=True),
    )
    routed, rows_in = (
        lax.all_gather(routed, "tp", axis=2, tiled=True),
        lax.all_gather(rows_in, "tp", axis=2, tiled=True),
    )
    width_d = routed.shape[-1]
    routed = routed.reshape(-1, width_d)
    rows_in = rows_in.reshape(-1, width_d)
    w_gate, w_up, w_down = (weight_gate[0], weight_up[0], weight_down[0])
    grad_gate, grad_up, grad_down, d_gate, d_up = expert_back(routed, rows_in, w_gate, w_up, w_down)
    across = (((1,), (1,)), ((), ()))
    partial_rows = lax.dot_general(d_gate, w_gate, across, preferred_element_type=jnp.float32)
    partial_rows = partial_rows + lax.dot_general(
        d_up, w_up, across, preferred_element_type=jnp.float32
    )
    summed = lax.psum_scatter(
        partial_rows.reshape(experts, capacity, width_d).astype(jnp.bfloat16),
        "tp",
        scatter_dimension=2,
        tiled=True,
    )
    returned = lax.all_to_all(summed, "sp", split_axis=0, concat_axis=0, tiled=True)
    gathered_back = jnp.dot(
        picker, returned.reshape(experts * capacity, -1), preferred_element_type=jnp.float32
    )
    residual_grad = (cotangent.astype(jnp.float32) + gathered_back).astype(jnp.bfloat16)
    shard_piece = lax.all_gather(residual_grad, "tp", axis=1, tiled=True)
    grad_mix = jnp.dot(shard_piece, out_weight, preferred_element_type=jnp.float32)
    grad_mix, whole = (grad_mix, shard_piece)
    grad_mix = grad_mix.astype(jnp.bfloat16)
    proj_grad = lax.psum_scatter(
        lax.dot_general(whole, mixer_out, contract, preferred_element_type=jnp.float32),
        "sp",
        scatter_dimension=0,
        tiled=True,
    )
    query_heads = heads_first(queries, DK)
    key_heads = heads_first(key_vectors, DK)
    value_heads = heads_first(values, DV)
    decay_heads = heads_first(log_decay, DK)
    out_grad = heads_first(grad_mix, DV)
    cumulative = jnp.cumsum(decay_heads, axis=1)
    device_total = cumulative[:, -1, :]
    decay_all = jnp.exp(device_total)
    carry_term = jnp.einsum(
        "hnd,hnv->hdv",
        key_heads * jnp.exp(device_total[:, None, :] - cumulative),
        value_heads,
        precision=HIGHEST,
    )
    back_term = jnp.einsum(
        "hnd,hnv->hdv",
        query_heads * DK ** (-0.5) * jnp.exp(cumulative),
        out_grad,
        precision=HIGHEST,
    )
    identity = (jnp.ones_like(decay_all), jnp.zeros_like(carry_term))
    entering = carried_in((decay_all, carry_term), "sp", join_states, identity, False)[1]
    leaving = carried_in((decay_all, back_term), "sp", join_states, identity, True)[1]

    def forward_here(query_in, key_in, value_in, decay_in):
        return local_forward(query_in, key_in, value_in, decay_in, entering)

    primal, pullback = jax.vjp(forward_here, query_heads, key_heads, value_heads, decay_heads)
    grad_q, grad_k, grad_v, grad_l = pullback((out_grad, leaving))
    return (
        grad_gate[None],
        grad_up[None],
        grad_down[None],
        proj_grad,
        tokens_first(grad_q).astype(jnp.bfloat16),
        tokens_first(grad_k).astype(jnp.bfloat16),
        tokens_first(grad_v).astype(jnp.bfloat16),
        tokens_first(grad_l),
    )


def solution(mesh):
    return jax.shard_map(
        shards,
        mesh=mesh,
        in_specs=(
            P("sp", "tp"),
            P("sp", "tp"),
            P("sp", None),
            P("sp"),
            P("sp", None),
            P("sp", None, "tp"),
            P("sp", None, "tp"),
            P("sp", "tp", None),
            P(None, "tp"),
            P("sp", "tp"),
            P("sp", "tp"),
            P("sp", "tp"),
            P("sp", "tp"),
            P("sp", "tp"),
        ),
        out_specs=(
            P("sp", None, "tp"),
            P("sp", None, "tp"),
            P("sp", "tp", None),
            P("sp", "tp"),
            P("sp", "tp"),
            P("sp", "tp"),
            P("sp", "tp"),
            P("sp", "tp"),
        ),
        check_vma=False,
    )
```

profile of v0, /device:TPU:0, one launch (start us, length us, event | category | flops | bytes accessed | tf_op | source)
XLA Modules:
  0.0 247.3 jit_solution(14660690588816724807)
XLA Ops:
  12.5 18.8 %all_to_all.15 = bf16[8,48,512]{2,1,0:T(8,128)(2,1)} all-to-all(bf16[8,48,512]{2,1,0:T(8,128)(2,1)S(1)} %bitcast.484), channel_id=1, replica_groups=mesh['sp'=8,'tp'=4] {'sp'}, dimensions={0} | all-to-all | bytes 786432 | tf_op jit(solution)/shard_map/all_to_all | solution.py:145
  32.1 15.6 %all_to_all.16 = bf16[8,48,512]{2,1,0:T(8,128)(2,1)} all-to-all(bf16[8,48,512]{2,1,0:T(8,128)(2,1)S(1)} %bitcast.483), channel_id=1, replica_groups=mesh['sp'=8,'tp'=4] {'sp'}, dimensions={0} | all-to-all | bytes 786432 | tf_op jit(solution)/shard_map/all_to_all | solution.py:144
  47.8 13.3 %all-gather.7.cloned.1.call-done = bf16[8,48,2048]{2,1,0:T(8,128)(2,1)} async-done(((bf16[8,48,512]{2,1,0:T(8,128)(2,1)}), bf16[8,48,2048]{2,1,0:T(8,128)(2,1)}) %all-gather.7.cloned.1.call-update) | async-done | bytes 1572880 | tf_op jit(solution)/shard_map/all_gather | solution.py:149
  63.8 29.8 %all-gather.9.cloned.1.call-done = bf16[8,48,2048]{2,1,0:T(8,128)(2,1)} async-done(((bf16[8,48,512]{2,1,0:T(8,128)(2,1)}), bf16[8,48,2048]{2,1,0:T(8,128)(2,1)}) %all-gather.9.cloned.1.call-update) | async-done | bytes 1572880 | tf_op jit(solution)/shard_map/all_gather | solution.py:148
  100.0 11.7 %all_gather.30 = f32[8,1,128]{2,1,0:T(1,128)S(1)} all-gather(f32[1,1,128]{2,1,0:T(1,128)S(1)} %get-tuple-element.1428), channel_id=1, replica_groups=mesh['sp'=8,'tp'=4] {'sp'}, dimensions={0}, use_global_device_ids=true | all-gather | bytes 4608 | tf_op jit(solution)/shard_map/all_gather | solution.py:19
  111.8 17.6 %reduce-scatter.3.cloned.1.call-done = bf16[8,48,512]{2,1,0:T(8,128)(2,1)} async-done(((bf16[8,48,2048]{2,1,0:T(8,128)(2,1)}), bf16[8,48,512]{2,1,0:T(8,128)(2,1)}) %reduce-scatter.3.cloned.1.call-update) | async-done | bytes 393232 | tf_op jit(solution)/shard_map/reduce_scatter | solution.py:161
  129.3 4.6 %all-to-all-start.2 = ((bf16[8,48,512]{2,1,0:T(8,128)(2,1)}), bf16[8,48,512]{2,1,0:T(8,128)(2,1)S(1)}, u32[]{:S(2)}, u32[]{:S(2)}) async-start(bf16[8,48,512]{2,1,0:T(8,128)(2,1)} %reduce-scatter.3.cloned.1.call-done), calls=%async_computation.3 | async-start | bytes 786432 | tf_op jit(solution)/shard_map/all_to_all | solution.py:167
  134.1 12.4 %all-to-all-done.2 = bf16[8,48,512]{2,1,0:T(8,128)(2,1)S(1)} async-done(((bf16[8,48,512]{2,1,0:T(8,128)(2,1)}), bf16[8,48,512]{2,1,0:T(8,128)(2,1)S(1)}, u32[]{:S(2)}, u32[]{:S(2)}) %all-to-all-start.2) | async-done | bytes 393248 | tf_op jit(solution)/shard_map/all_to_all | solution.py:167
  146.7 10.4 %all_gather.29 = bf16[128,2048]{1,0:T(8,128)(2,1)S(1)} all-gather(bf16[128,512]{1,0:T(8,128)(2,1)S(1)} %fusion.76), channel_id=1, replica_groups=mesh['sp'=8,'tp'=4] {'tp'}, dimensions={1}, use_global_device_ids=true | all-gather | bytes 655360 | tf_op jit(solution)/shard_map/all_gather | solution.py:172
  158.7 38.7 %while.91 = (s32[]{:T(128)}, f32[1,128,256]{2,1,0:T(8,128)S(1)}, f32[2,1,64,128]{3,2,1,0:T(8,128)S(1)}, f32[2,1,64,128]{3,2,1,0:T(8,128)S(1)}, f32[2,1,64,128]{3...) while((s32[]{:T(128)}, f32[1,128,256]{2,1,0:T(8,128)S(1)}, ...), condition=%wide.region_14.15_spmd.clone.clone, body=%wide.region_12.14_spmd.clone.clone.sunk | while | flops 31035392 | bytes 28814028 | solution.py:59
  160.1 2.9 %select_dynamic-update-slice_fusion.2 = (f32[2,1,64,64,128]{4,3,2,1,0:T(8,128)}, f32[2,1,64,64,128]{4,3,2,1,0:T(8,128)}) fusion(f32[2,1,64,64,128]{4,3,2,1,0:T(8,128)} %get-tuple-element.1860, s32[]{:T(128)S(6)} %copy.169, f32[64,128]{1,0:T(8,128)S(1)} %bitcast.474, pred[64,64]{1,0:T(8,128)(4,1)S(1)} %get-tuple-element.1892, ...), kind=kLoop, calls=%fused_computation.11.clone.1 | loop fusion | flops 1572864 | bytes 4268036 | tf_op jit(solution)/shard_map/jvp()/while/body/jit(dynamic_update_index_in_dim)/dynamic_update_slice | solution.py:59
  165.8 3.5 %copy.123 = f32[1,1,64,128,64]{3,2,4,1,0:T(8,128)S(1)} copy(f32[1,1,64,128,64]{4,3,2,1,0:T(8,128)} %multiply_bitcast_fusion.3) | data formatting | bytes 4194304 | tf_op jit(solution)/shard_map/jvp()/while/body/jit(dynamic_update_index_in_dim)/dynamic_update_slice | solution.py:59
  171.5 2.8 %copy.124 = f32[64,64,128]{0,2,1:T(8,128)} copy(f32[64,64,128]{2,1,0:T(8,128)S(1)} %exponential_select_fusion.2) | data formatting | bytes 4194304 | tf_op jit(solution)/shard_map/jvp()/while
  174.3 3.0 %fusion.162 = f32[64,64]{0,1:T(8,128)S(1)} fusion(f32[64,64,128]{0,2,1:T(8,128)} %copy.124, f32[128,64]{1,0:T(8,128)S(1)} %copy.122, f32[128,64]{0,1:T(8,128)S(1)} %get-tuple-element.1746), kind=kLoop, calls=%fused_computation.9.clone.1 | loop fusion | flops 1568768 | bytes 2179072 | tf_op jit(solution)/shard_map/jvp()/while
  179.4 2.9 %select_dynamic-update-slice_fusion.2 = (f32[2,1,64,64,128]{4,3,2,1,0:T(8,128)}, f32[2,1,64,64,128]{4,3,2,1,0:T(8,128)}) fusion(f32[2,1,64,64,128]{4,3,2,1,0:T(8,128)} %get-tuple-element.1860, s32[]{:T(128)S(6)} %copy.169, f32[64,128]{1,0:T(8,128)S(1)} %bitcast.474, pred[64,64]{1,0:T(8,128)(4,1)S(1)} %get-tuple-element.1892, ...), kind=kLoop, calls=%fused_computation.11.clone.1 | loop fusion | flops 1572864 | bytes 4268036 | tf_op jit(solution)/shard_map/jvp()/while/body/jit(dynamic_update_index_in_dim)/dynamic_update_slice | solution.py:59
  185.1 3.5 %copy.123 = f32[1,1,64,128,64]{3,2,4,1,0:T(8,128)S(1)} copy(f32[1,1,64,128,64]{4,3,2,1,0:T(8,128)} %multiply_bitcast_fusion.3) | data formatting | bytes 4194304 | tf_op jit(solution)/shard_map/jvp()/while/body/jit(dynamic_update_index_in_dim)/dynamic_update_slice | solution.py:59
  190.8 2.7 %copy.124 = f32[64,64,128]{0,2,1:T(8,128)} copy(f32[64,64,128]{2,1,0:T(8,128)S(1)} %exponential_select_fusion.2) | data formatting | bytes 4194304 | tf_op jit(solution)/shard_map/jvp()/while
  193.6 3.0 %fusion.162 = f32[64,64]{0,1:T(8,128)S(1)} fusion(f32[64,64,128]{0,2,1:T(8,128)} %copy.124, f32[128,64]{1,0:T(8,128)S(1)} %copy.122, f32[128,64]{0,1:T(8,128)S(1)} %get-tuple-element.1746), kind=kLoop, calls=%fused_computation.9.clone.1 | loop fusion | flops 1568768 | bytes 2179072 | tf_op jit(solution)/shard_map/jvp()/while
  197.5 3.0 %fusion.72 = bf16[1,2048,128]{2,1,0:T(8,128)(2,1)} fusion(bf16[384,2048]{1,0:T(8,128)(2,1)} %bitcast.477, bf16[384,128]{1,0:T(8,128)(2,1)} %copy-done.42), kind=kOutput, calls=%fused_computation.121 | convolution fusion | flops 201588736 | bytes 2195456 | tf_op jit(solution)/shard_map/dot_general | solution.py:92
  206.2 7.4 %while.89 = (s32[]{:T(128)}, f32[1,128,256]{2,1,0:T(8,128)S(1)}, s32[]{:T(128)}, f32[8,1,128]{2,1,0:T(1,128)S(1)}, f32[8,1,128,256]{3,2,1,0:T(8,128)}, /*index=5*/s32[]{:T(128)}, s32[]{:T(128)}, s32[]{:T(128)}, s32[]{:T(128)}) while((s32[]{:T(128)}, f32[1,128,256]{2,1,0:T(8,128)S(1)}, s32[]{:T(128)}, f32[8,1,128]{2,1,0:T(1,128)S(1)}, ...), condition=%wide.region_9.10_spmd, body=%wide.region_8.9_spmd.sunk | while | flops 65542 | bytes 394907 | solution.py:28
  213.8 19.3 %while.92 = (s32[]{:T(128)}, f32[1,128,256]{1,2,0:T(8,128)S(1)}, bf16[2,1,64,128]{3,2,1,0:T(8,128)(2,1)S(1)}, bf16[2,1,64,128]{3,2,1,0:T(8,128)(2,1)S(1)}, bf16[...) while((s32[]{:T(128)}, f32[1,128,256]{1,2,0:T(8,128)S(1)}, ...), condition=%wide.region_21.22_spmd.clone.clone, body=%wide.region_15.21_spmd.clone.clone.sunk | while | flops 132898816 | bytes 28491060 | solution.py:59
  219.9 3.2 %fusion.182 = (f32[64,128]{1,0:T(8,128)S(1)}, f32[64,128]{1,0:T(8,128)S(1)}) fusion(f32[2,1,64,64,128]{4,3,2,1,0:T(8,128)S(1)} %copy-done.1, s32[]{:T(128)S(6)} %sub.212, f32[2,1,64,128,64]{3,2,4,1,0:T(8,128)} %get-tuple-element.1961, f32[64,64]{1,0:T(8,128)S(1)} %fusion.173, pred[64,64]{1,0:T(8,128)(4,1)S(1)} %get-tuple-element.1964), kind=kLoop, calls=%fused_computation.58.clone.1 | loop fusion | flops 3129344 | bytes 4280324 | tf_op jit(solution)/shard_map/transpose(jvp())/while/body/eval_jaxpr/reduce_sum | solution.py:47
  229.6 3.2 %fusion.182 = (f32[64,128]{1,0:T(8,128)S(1)}, f32[64,128]{1,0:T(8,128)S(1)}) fusion(f32[2,1,64,64,128]{4,3,2,1,0:T(8,128)S(1)} %copy-done.1, s32[]{:T(128)S(6)} %sub.212, f32[2,1,64,128,64]{3,2,4,1,0:T(8,128)} %get-tuple-element.1961, f32[64,64]{1,0:T(8,128)S(1)} %fusion.173, pred[64,64]{1,0:T(8,128)(4,1)S(1)} %get-tuple-element.1964), kind=kLoop, calls=%fused_computation.58.clone.1 | loop fusion | flops 3129344 | bytes 4280324 | tf_op jit(solution)/shard_map/transpose(jvp())/while/body/eval_jaxpr/reduce_sum | solution.py:47
  233.2 6.7 %reduce-scatter.5.cloned.1.call-done = f32[256,256]{1,0:T(8,128)} async-done(((f32[2048,256]{1,0:T(8,128)}), f32[256,256]{1,0:T(8,128)}) %reduce-scatter.5.cloned.1.call-update) | async-done | bytes 262160 | tf_op jit(solution)/shard_map/reduce_scatter | solution.py:176
  (309 shorter events, 55.3 us)
Async XLA Ops:
  8.0 149.1 %copy-start = (bf16[2048,256]{1,0:T(8,128)(2,1)S(1)}, bf16[2048,256]{1,0:T(8,128)(2,1)}, u32[]{:S(2)}) copy-start(bf16[2048,256]{1,0:T(8,128)(2,1)} %param.30) | copy-start | bytes 3145732
  8.0 23.3 %copy-start.55 = (f32[128,2]{0,1:T(2,128)S(1)}, f32[128,2]{0,1:T(2,128)}, u32[]{:S(2)}) copy-start(f32[128,2]{0,1:T(2,128)} %param.26) | copy-start | bytes 3076
  8.0 23.3 %copy-start.56 = (f32[128]{0:T(128)S(1)}, f32[128]{0:T(128)}, u32[]{:S(2)}) copy-start(f32[128]{0:T(128)} %param.25) | copy-start | bytes 1540
  8.0 23.8 %copy-start.38 = (bf16[128,512]{1,0:T(8,128)(2,1)S(1)}, bf16[128,512]{1,0:T(8,128)(2,1)}, u32[]{:S(2)}) copy-start(bf16[128,512]{1,0:T(8,128)(2,1)} %param.22) | copy-start | bytes 393220
  8.0 53.0 %copy-start.19 = (bf16[1,2048,128]{2,1,0:T(8,128)(2,1)S(1)}, bf16[1,2048,128]{2,1,0:T(8,128)(2,1)}, u32[]{:S(2)}) copy-start(bf16[1,2048,128]{2,1,0:T(8,128)(2,1)} %param.27) | copy-start | bytes 1572868
  8.1 53.0 %all-gather.7.cloned.1.call-start = ((), (), s32[]{:S(2)}) async-start(), calls=%async_computation.5 | async-start | bytes 1966080 | tf_op jit(solution)/shard_map/all_gather | solution.py:149
  31.3 62.4 %all-gather.9.cloned.1.call-start = ((), (), s32[]{:S(2)}) async-start(), calls=%async_computation.6 | async-start | bytes 1966080 | tf_op jit(solution)/shard_map/all_gather | solution.py:148
  31.4 31.9 %copy-start.20 = (bf16[1,2048,128]{2,1,0:T(8,128)(2,1)S(1)}, bf16[1,2048,128]{2,1,0:T(8,128)(2,1)}, u32[]{:S(2)}) copy-start(bf16[1,2048,128]{2,1,0:T(8,128)(2,1)} %param.28) | copy-start | bytes 1572868
  47.7 81.6 %reduce-scatter.3.cloned.1.call-start = ((), (), s32[]{:S(2)}) async-start(), calls=%async_computation.7 | async-start | bytes 1966080 | tf_op jit(solution)/shard_map/reduce_scatter | solution.py:161
  61.1 32.6 %copy-start.57 = (bf16[1,128,2048]{2,1,0:T(8,128)(2,1)S(1)}, bf16[1,128,2048]{2,1,0:T(8,128)(2,1)}, u32[]{:S(2)}) copy-start(bf16[1,128,2048]{2,1,0:T(8,128)(2,1)} %param.29) | copy-start | bytes 1572868
  63.2 32.4 %copy-start.32 = (f32[384,128]{1,0:T(8,128)}, f32[384,128]{1,0:T(8,128)S(1)}, u32[]{:S(2)}) copy-start(f32[384,128]{1,0:T(8,128)S(1)} %fusion.79) | copy-start | bytes 589828
  63.8 32.4 %copy-start.34 = (f32[384,128]{1,0:T(8,128)}, f32[384,128]{1,0:T(8,128)S(1)}, u32[]{:S(2)}) copy-start(f32[384,128]{1,0:T(8,128)S(1)} %fusion.82) | copy-start | bytes 589828
  98.0 36.0 %all-gather.13.cloned.1.call-start = ((), (), s32[]{:S(2)}) async-start(), calls=%async_computation.10 | async-start | bytes 1179648 | tf_op jit(solution)/shard_map/all_gather | solution.py:19
  99.3 34.7 %copy-start.47 = (bf16[2,1,64,128]{3,2,1,0:T(8,128)(2,1)}, bf16[2,1,64,128]{3,2,1,0:T(8,128)(2,1)S(1)}, u32[]{:S(2)}) copy-start(bf16[2,1,64,128]{3,2,1,0:T(8,128)(2,1)S(1)} %fusion.106) | copy-start | bytes 98308
  129.3 17.1 %all-to-all-start.2 = ((bf16[8,48,512]{2,1,0:T(8,128)(2,1)}), bf16[8,48,512]{2,1,0:T(8,128)(2,1)S(1)}, u32[]{:S(2)}, u32[]{:S(2)}) async-start(bf16[8,48,512]{2,1,0:T(8,128)(2,1)} %reduce-scatter.3.cloned.1.call-done), calls=%async_computation.3 | async-start | bytes 786432 | tf_op jit(solution)/shard_map/all_to_all | solution.py:167
  133.9 72.2 %all-gather.11.cloned.1.call-start = ((), (), s32[]{:S(2)}) async-start(), calls=%async_computation.9 | async-start | bytes 1179648 | tf_op jit(solution)/shard_map/all_gather | solution.py:19
  158.4 81.5 %reduce-scatter.5.cloned.1.call-start = ((), (), s32[]{:S(2)}) async-start(), calls=%async_computation.8 | async-start | bytes 2359296 | tf_op jit(solution)/shard_map/reduce_scatter | solution.py:176
  206.1 7.7 %copy-start.14 = (f32[2,1,64,128]{3,2,1,0:T(8,128)S(1)}, f32[2,1,64,128]{3,2,1,0:T(8,128)}, u32[]{:S(2)}) copy-start(f32[2,1,64,128]{3,2,1,0:T(8,128)} %copy-done.13) | copy-start | bytes 196612
  206.1 7.7 %copy-start.18 = (f32[2,1,64,128]{3,2,1,0:T(8,128)S(1)}, f32[2,1,64,128]{3,2,1,0:T(8,128)}, u32[]{:S(2)}) copy-start(f32[2,1,64,128]{3,2,1,0:T(8,128)} %copy-done.17) | copy-start | bytes 196612
  206.1 7.7 %copy-start.27 = (f32[2,1,64,128]{3,2,1,0:T(8,128)S(1)}, f32[2,1,64,128]{3,2,1,0:T(8,128)}, u32[]{:S(2)}) copy-start(f32[2,1,64,128]{3,2,1,0:T(8,128)} %copy-done.26) | copy-start | bytes 196612
  206.1 7.7 %copy-start.41 = (f32[2,1,64,64]{3,2,1,0:T(8,128)S(1)}, f32[2,1,64,64]{3,2,1,0:T(8,128)}, u32[]{:S(2)}) copy-start(f32[2,1,64,64]{3,2,1,0:T(8,128)} %get-tuple-element.1995) | copy-start | bytes 98308
  206.1 7.7 %copy-start.48 = (bf16[2,1,64,128]{3,2,1,0:T(8,128)(2,1)S(1)}, bf16[2,1,64,128]{3,2,1,0:T(8,128)(2,1)}, u32[]{:S(2)}) copy-start(bf16[2,1,64,128]{3,2,1,0:T(8,128)(2,1)} %copy-done.47) | copy-start | bytes 98308
  206.1 7.7 %copy-start.53 = (bf16[2,1,64,128]{3,2,1,0:T(8,128)(2,1)S(1)}, bf16[2,1,64,128]{3,2,1,0:T(8,128)(2,1)}, u32[]{:S(2)}) copy-start(bf16[2,1,64,128]{3,2,1,0:T(8,128)(2,1)} %copy.200) | copy-start | bytes 98308
  206.1 7.7 %copy-start.60 = (f32[2,1,128,1]{2,3,1,0:T(1,128)S(1)}, f32[2,1,128,1]{2,3,1,0:T(1,128)}, u32[]{:S(2)}) copy-start(f32[2,1,128,1]{2,3,1,0:T(1,128)} %get-tuple-element.1999) | copy-start | bytes 3076
  (62 other events, 231.8 us)
Sparse Core Ops, SparseCore 0:
  31.4 29.6 all-gather.6
  62.9 30.6 all-gather.8
  98.2 31.1 reduce-scatter.2
Sparse Core Ops, SparseCore 1:
  100.7 22.1 all-gather.12
  158.5 19.6 all-gather.10
  206.2 33.6 reduce-scatter.4
where the time goes:
time: 248 us; the launch traced here: 247 us
  waiting for transfers between devices  79.9 us (32%)
  blocking collectives  56.5 us (23%)
  other arithmetic  43.1 us (17%)
  matrix products  23.4 us (9%)
  local copies, waits for them, and re-layouts  22 us (9%)
  between operations  16.3 us (7%)
  starting transfers between devices  5.04 us (2%)
    all_gather x1, waiting for transfers between devices, shards(): lax.all_gather(routed, 'tp', axis=2, tiled=True)  29.8 us
    all_to_all x1, blocking collectives, shards(): lax.all_to_all(rows_in, 'sp', split_axis=0, concat_axis=0, tiled=True)  18.8 us
    reduce_scatter x1, waiting for transfers between devices, shards(): lax.psum_scatter(partial_rows.reshape(experts, capacity, width_d).astype(...  17.6 us
    all_to_all x1, blocking collectives, shards(): lax.all_to_all(routed, 'sp', split_axis=0, concat_axis=0, tiled=True)  15.6 us
    all_gather x1, waiting for transfers between devices, shards(): lax.all_gather(rows_in, 'tp', axis=2, tiled=True)  13.3 us
    all_to_all x1, waiting for transfers between devices, shards(): lax.all_to_all(summed, 'sp', split_axis=0, concat_axis=0, tiled=True)  12.4 us
    all_gather x1, blocking collectives, carried_in(): gathered = jax.tree.map(lambda a: lax.all_gather(a, axis), part)  11.7 us
    dynamic_update_slice x14, local copies, waits for them, and re-layouts, local_forward(): lax.scan(block_step, state_in, (blocked(query_heads), blocked(key_heads),...  11.6 us
  transfers between devices with their start and end apart: 7, of which 5 were waited for; matrix products, arithmetic and copies ran while one was open for 31% of the time, Pallas kernels for 0%

commit v1 on v0

v1 whole, which is shorter than its diff:
```python
import functools
import math

import jax
import jax.numpy as jnp
from jax import lax
from jax.experimental import pallas as pl
from jax.experimental.pallas import tpu as pltpu
from jax.sharding import PartitionSpec as P

DK = 128
DV = 256
TOK = 128
BLK = 64
HIGHEST = lax.Precision.HIGHEST
F32 = jnp.float32
BF16 = jnp.bfloat16
MESH = pl.DeviceIdType.MESH


def tp_grid(n_tp):
    cols = math.isqrt(n_tp)
    while n_tp % cols:
        cols -= 1
    return n_tp // cols, cols


def sp_order(n_sp):
    if n_sp % 2:
        return [(d, 0) for d in range(1, n_sp)], n_sp, 1
    z = n_sp // 2
    places = [(dz, dc) for dz in range(z) for dc in range(2)][1:]
    places.sort(key=lambda p: (min(p[0], z - p[0]), p))
    return places, z, 2


class Place:
    def __init__(self, n_sp, n_tp):
        self.n_sp, self.n_tp = n_sp, n_tp
        self.sp, self.tp = lax.axis_index("sp"), lax.axis_index("tp")
        self.order, self.z, self.cores = sp_order(n_sp)
        self.rows, self.cols = tp_grid(n_tp)

    def sp_peer(self, place, back=False):
        dz, dc = place
        zz, cc = self.sp // self.cores, self.sp % self.cores
        if back:
            dz, dc = self.z - dz, self.cores - dc
        return ((zz + dz) % self.z) * self.cores + (cc + dc) % self.cores

    def row_peer(self, off):
        r, c = self.tp // self.cols, self.tp % self.cols
        return r * self.cols + (c + off) % self.cols

    def col_peer(self, off):
        r, c = self.tp // self.cols, self.tp % self.cols
        return ((r + off) % self.rows) * self.cols + c

    def tp_peer(self, off):
        return (self.tp + off) % self.n_tp


def send(src, dst, send_sem, recv_sem, sp, tp):
    copy = pltpu.make_async_remote_copy(
        src_ref=src, dst_ref=dst, send_sem=send_sem, recv_sem=recv_sem,
        device_id=(sp, tp), device_id_type=MESH,
    )
    copy.start()


def wait_bytes(ref, sem):
    pltpu.make_async_copy(ref, ref, sem).wait()


def meet(here):
    barrier = pltpu.get_barrier_semaphore()
    for place in here.order:
        pl.semaphore_signal(
            barrier, inc=1, device_id=(here.sp_peer(place), here.tp), device_id_type=MESH
        )
    for off in range(1, here.n_tp):
        pl.semaphore_signal(
            barrier, inc=1, device_id=(here.sp, here.tp_peer(off)), device_id_type=MESH
        )
    pl.semaphore_wait(barrier, here.n_sp + here.n_tp - 2)


def at(start, size):
    return pl.ds(pl.multiple_of(start * size, size), size)


def dispatch_kernel(
    n_sp, n_tp, routed, rows_in, mixer, out_routed, out_rows, mixer_all,
    sp_send, sp_recv, one_send, one_recv, two_send, two_recv, mix_send, mix_recv,
):
    here = Place(n_sp, n_tp)
    cap, width = routed.shape[0] // n_sp, routed.shape[1]
    tok = mixer.shape[0]
    meet(here)
    pairs = ((0, routed, out_routed), (1, rows_in, out_rows))
    for a, src, dst in pairs:
        for k, place in enumerate(here.order):
            peer = here.sp_peer(place)
            send(
                src.at[at(peer, cap)], dst.at[at(here.sp, cap), at(here.tp, width)],
                sp_send.at[a], sp_recv.at[a, k], peer, here.tp,
            )

    def spread(a, k, source, block, dst):
        firsts = range(1, here.cols if a == 0 else here.rows)
        seconds = range(1, here.rows if a == 0 else here.cols)
        first_peer = here.row_peer if a == 0 else here.col_peer
        second_peer = here.col_peer if a == 0 else here.row_peer
        target = dst.at[at(source, cap), at(here.tp, width)]
        for off in firsts:
            send(
                block, target, one_send.at[a], one_recv.at[a, k, off - 1],
                here.sp, first_peer(off),
            )
        for off in seconds:
            send(block, target, two_send.at[a], two_recv.at[a], here.sp, second_peer(off))

    def relay(a, k, source, dst):
        firsts = range(1, here.cols if a == 0 else here.rows)
        seconds = range(1, here.rows if a == 0 else here.cols)
        first_peer = here.row_peer if a == 0 else here.col_peer
        second_peer = here.col_peer if a == 0 else here.row_peer
        size = here.cols if a == 0 else here.rows
        for off in firsts:
            block = dst.at[at(source, cap), at(first_peer(size - off), width)]
            wait_bytes(block, one_recv.at[a, k, off - 1])
            for soff in seconds:
                send(block, block, two_send.at[a], two_recv.at[a], here.sp, second_peer(soff))

    last = len(here.order)
    for a, src, dst in pairs:
        spread(a, last, here.sp, src.at[at(here.sp, cap)], dst)
    for place in here.order:
        send(
            mixer, mixer_all.at[at(here.sp, tok)], mix_send.at[0], mix_recv.at[0],
            here.sp_peer(place), here.tp,
        )
    for a, src, dst in pairs:
        dst[at(here.sp, cap), at(here.tp, width)] = src[at(here.sp, cap), :]
    mixer_all[at(here.sp, tok), :] = mixer[...]
    sources = [here.sp_peer(place, back=True) for place in here.order] + [here.sp]
    steps = [last] + list(range(last))
    for i, k in enumerate(steps):
        if i + 1 < len(steps):
            k_next = steps[i + 1]
            for a, src, dst in pairs:
                block = dst.at[at(sources[k_next], cap), at(here.tp, width)]
                wait_bytes(block, sp_recv.at[a, k_next])
                spread(a, k_next, sources[k_next], block, dst)
        for a, src, dst in pairs:
            relay(a, k, sources[k], dst)
    for a, src, dst in pairs:
        count = here.cols - 1 if a == 0 else here.rows - 1
        twos = (here.rows - 1 if a == 0 else here.cols - 1) * (1 + count)
        wait_bytes(dst.at[:, pl.ds(0, twos * width)], two_recv.at[a])
        wait_bytes(dst.at[:, pl.ds(0, twos * width)], two_send.at[a])
        wait_bytes(dst.at[:, pl.ds(0, count * width)], one_send.at[a])
        wait_bytes(src.at[pl.ds(0, (n_sp - 1) * cap)], sp_send.at[a])
    wait_bytes(mixer_all.at[pl.ds(0, (n_sp - 1) * tok)], mix_recv.at[0])
    wait_bytes(mixer_all.at[pl.ds(0, (n_sp - 1) * tok)], mix_send.at[0])


def mm(a, b, ca, cb, precision=HIGHEST):
    return lax.dot_general(
        a, b, (((ca,), (cb,)), ((), ())), precision=precision, preferred_element_type=F32
    )


def triangle(size, lower):
    rows = lax.broadcasted_iota(jnp.int32, (size, size), 0)
    cols = lax.broadcasted_iota(jnp.int32, (size, size), 1)
    return rows >= cols if lower else rows <= cols


def return_kernel(
    n_sp, n_tp, parts, picker, cotangent, out_weight, queries, keys, values, decay, mixer_all,
    proj, grad_q, grad_k, grad_v, grad_l,
    got, summed, returned, piece, piece_t, pieces, carry, carries, total, totals, back, backs,
    state,
    tp_send, tp_recv, sp_send, sp_recv, piece_send, piece_recv, carry_send, carry_recv,
    total_send, total_recv, back_send, back_recv, res_send, res_recv,
):
    here = Place(n_sp, n_tp)
    me = here.sp
    cap, width = parts.shape[0] // n_sp, cotangent.shape[1]
    tok, blocks = queries.shape[0], queries.shape[0] // BLK
    out_rows = proj.shape[0]
    meet(here)
    order = list(reversed(here.order))
    for k, place in enumerate(order):
        peer = here.sp_peer(place)
        for off in range(1, n_tp):
            send(
                parts.at[at(peer, cap), at(here.tp_peer(off), width)],
                got.at[off - 1, at(peer, cap)],
                tp_send.at[0], tp_recv.at[k], me, here.tp_peer(off),
            )
    for off in range(1, n_tp):
        send(
            parts.at[at(me, cap), at(here.tp_peer(off), width)],
            got.at[off - 1, at(me, cap)],
            tp_send.at[0], tp_recv.at[n_sp - 1], me, here.tp_peer(off),
        )

    scale = DK ** (-0.5)
    lower = triangle(BLK, True)
    ones = jnp.where(lower, 1.0, 0.0).astype(F32)
    cums, ends = [], []
    for b in range(blocks):
        cum = mm(ones, decay[b * BLK:(b + 1) * BLK, :], 1, 0)
        cums.append(cum)
        ends.append(cum[BLK - 1:BLK, :])
    span = sum(ends[1:], ends[0])
    term = None
    for b in range(blocks):
        rows = slice(b * BLK, (b + 1) * BLK)
        key_end = keys[rows, :].astype(F32) * jnp.exp(ends[b] - cums[b])
        fresh = mm(values[rows, :].astype(F32), key_end, 0, 0)
        term = fresh if term is None else jnp.exp(ends[b]) * term + fresh
    carry[...] = term.astype(BF16)
    total[...] = jnp.broadcast_to(span, total.shape)
    for k, place in enumerate(here.order):
        peer = here.sp_peer(place)
        send(
            total, totals.at[me], total_send.at[0], total_recv.at[0], peer, here.tp
        )

        @pl.when(peer > me)
        def _():
            send(carry, carries.at[me], carry_send.at[k], carry_recv.at[k], peer, here.tp)

    for k, place in enumerate(order + [None]):
        source = me if place is None else here.sp_peer(place)
        wait_bytes(got.at[:, at(source, cap)], tp_recv.at[k])
        value = parts[at(source, cap), at(here.tp, width)].astype(F32)
        for off in range(1, n_tp):
            value = value + got[off - 1, at(source, cap), :].astype(F32)
        if place is None:
            returned[at(me, cap), :] = value.astype(BF16)
        else:
            summed[at(source, cap), :] = value.astype(BF16)
            send(
                summed.at[at(source, cap)], returned.at[at(me, cap)],
                sp_send.at[0], sp_recv.at[0], source, here.tp,
            )
    wait_bytes(returned.at[pl.ds(0, (n_sp - 1) * cap)], sp_recv.at[0])
    rowgrad = jnp.dot(picker[...], returned[...], preferred_element_type=F32)
    residual = (cotangent[...].astype(F32) + rowgrad).astype(BF16)
    piece[:, at(here.tp, width)] = residual
    for off in range(1, n_tp):
        send(
            piece.at[:, at(here.tp, width)], piece.at[:, at(here.tp, width)],
            piece_send.at[0], piece_recv.at[0], me, here.tp_peer(off),
        )

    wait_bytes(totals.at[pl.ds(0, n_sp - 1)], total_recv.at[0])
    totals[me] = total[...]
    for k, place in enumerate(here.order):
        source = here.sp_peer(place, back=True)

        @pl.when(source < me)
        def _():
            wait_bytes(carry, carry_recv.at[k])

    state[...] = jnp.zeros_like(state)
    for s in range(n_sp):
        @pl.when(s < me)
        def _():
            state[...] = jnp.exp(totals[s, 0:1, :]) * state[...] + carries[s].astype(F32)

    states = [state[...]]
    for b in range(blocks):
        rows = slice(b * BLK, (b + 1) * BLK)
        key_end = keys[rows, :].astype(F32) * jnp.exp(ends[b] - cums[b])
        states.append(
            jnp.exp(ends[b]) * states[b] + mm(values[rows, :].astype(F32), key_end, 0, 0)
        )

    wait_bytes(piece.at[:, pl.ds(0, (n_tp - 1) * width)], piece_recv.at[0])
    whole = piece[...]
    mix = jnp.dot(whole, out_weight[...], preferred_element_type=F32).astype(BF16).astype(F32)
    term = None
    for b in reversed(range(blocks)):
        rows = slice(b * BLK, (b + 1) * BLK)
        query_dec = queries[rows, :].astype(F32) * (scale * jnp.exp(cums[b]))
        fresh = mm(mix[rows, :], query_dec, 0, 0)
        term = fresh if term is None else jnp.exp(ends[b]) * term + fresh
    back[...] = term.astype(BF16)
    for k, place in enumerate(here.order):
        peer = here.sp_peer(place)

        @pl.when(peer < me)
        def _():
            send(back, backs.at[me], back_send.at[k], back_recv.at[k], peer, here.tp)

    piece_t[...] = whole.T
    for place in here.order:
        peer = here.sp_peer(place)
        send(
            piece_t.at[at(peer, out_rows)], pieces.at[me],
            res_send.at[0], res_recv.at[0], peer, here.tp,
        )

    kept = []
    for b in range(blocks):
        rows = slice(b * BLK, (b + 1) * BLK)
        grow, shrink = jnp.exp(cums[b]), jnp.exp(-cums[b])
        query_dec = queries[rows, :].astype(F32) * (scale * grow)
        key_dec = keys[rows, :].astype(F32) * shrink
        value, d_out = values[rows, :].astype(F32), mix[rows, :]
        scores = jnp.where(lower, mm(query_dec, key_dec, 1, 1), 0.0)
        d_scores = jnp.where(lower, mm(d_out, value, 1, 1), 0.0)
        d_query = (scale * grow) * (mm(d_out, states[b], 1, 0) + mm(d_scores, key_dec, 1, 0))
        d_key = shrink * mm(d_scores, query_dec, 0, 0)
        d_value = mm(scores, d_out, 0, 0)
        grad_q[rows, :] = d_query.astype(BF16)
        kept.append((d_query, d_key, d_value))

    for k, place in enumerate(here.order):
        source = here.sp_peer(place, back=True)

        @pl.when(source > me)
        def _():
            wait_bytes(back, back_recv.at[k])

    state[...] = jnp.zeros_like(state)
    for s in reversed(range(n_sp)):
        @pl.when(s > me)
        def _():
            state[...] = jnp.exp(totals[s, 0:1, :]) * state[...] + backs[s].astype(F32)

    leaving = state[...]
    edge = jnp.sum(states[blocks] * leaving, axis=0, keepdims=True)
    terms = [None] * blocks
    for b in reversed(range(blocks)):
        rows = slice(b * BLK, (b + 1) * BLK)
        query, key, value = queries[rows, :].astype(F32), keys[rows, :].astype(F32), values[rows, :].astype(F32)
        fall = jnp.exp(ends[b] - cums[b])
        d_query, d_key, d_value = kept[b]
        d_key = d_key + fall * mm(value, leaving, 1, 0)
        d_value = d_value + mm(key * fall, leaving, 1, 1)
        grad_k[rows, :] = d_key.astype(BF16)
        grad_v[rows, :] = d_value.astype(BF16)
        terms[b] = query * d_query - key * d_key
        if b:
            query_dec = query * (scale * jnp.exp(cums[b]))
            leaving = jnp.exp(ends[b]) * leaving + mm(mix[rows, :], query_dec, 0, 0)
    upper = jnp.where(triangle(BLK, False), 1.0, 0.0).astype(F32)
    for b in reversed(range(blocks)):
        rows = slice(b * BLK, (b + 1) * BLK)
        grad_l[rows, :] = mm(upper, terms[b], 1, 0) + edge
        edge = edge + jnp.sum(terms[b], axis=0, keepdims=True)

    wait_bytes(pieces.at[pl.ds(0, n_sp - 1)], res_recv.at[0])
    pieces[me] = piece_t[at(me, out_rows), :]
    acc = jnp.zeros(proj.shape, F32)
    for s in range(n_sp):
        acc = acc + jnp.dot(
            pieces[s], mixer_all[s * tok:(s + 1) * tok, :], preferred_element_type=F32
        )
    proj[...] = acc

    wait_bytes(got, tp_send.at[0])
    wait_bytes(returned.at[pl.ds(0, (n_sp - 1) * cap)], sp_send.at[0])
    wait_bytes(piece.at[:, pl.ds(0, (n_tp - 1) * width)], piece_send.at[0])
    wait_bytes(totals.at[pl.ds(0, n_sp - 1)], total_send.at[0])
    wait_bytes(pieces.at[pl.ds(0, n_sp - 1)], res_send.at[0])
    for k, place in enumerate(here.order):
        peer = here.sp_peer(place)

        @pl.when(peer > me)
        def _():
            wait_bytes(carry, carry_send.at[k])

        @pl.when(peer < me)
        def _():
            wait_bytes(back, back_send.at[k])


def vmem():
    return pl.BlockSpec(memory_space=pltpu.VMEM)


def shards(
    n_sp, n_tp,
    cotangent, moe_input, expert_ids, group_gate, expert_gate, weight_gate, weight_up,
    weight_down, out_weight, mixer_out, queries, key_vectors, values, log_decay,
):
    tokens, width = cotangent.shape
    width_d = width * n_tp
    experts = n_sp
    capacity = -(-max(2, 3 * TOK // experts) // 16) * 16
    slots = experts * capacity
    flat_ids = expert_ids.reshape(-1)
    onehot = (flat_ids[:, None] == jnp.arange(experts, dtype=jnp.int32)[None, :]).astype(jnp.int32)
    before = jnp.cumsum(onehot, axis=0) - onehot
    position = jnp.sum(before * onehot, axis=1)
    slot_index = flat_ids * capacity + position
    slot_match = slot_index[:, None] == jnp.arange(slots, dtype=jnp.int32)[None, :]
    route_weight = (group_gate[:, None] * expert_gate).reshape(-1)
    slot_weight = jnp.sum(jnp.where(slot_match, route_weight[:, None], 0.0), axis=0)
    picker = jnp.any(slot_match.reshape(tokens, 2, -1), axis=1).astype(BF16)
    contract = (((0,), (0,)), ((), ()))
    pulled_grad = lax.dot_general(picker, cotangent, contract, preferred_element_type=F32)
    rows_in = lax.dot_general(picker, moe_input, contract, preferred_element_type=F32).astype(BF16)
    routed = (slot_weight[:, None] * pulled_grad).astype(BF16)

    dma, rows_tp, cols_tp = pltpu.SemaphoreType.DMA, *tp_grid(n_tp)
    ones = max(rows_tp, cols_tp) - 1
    routed, rows_in, mixer_all = pl.pallas_call(
        functools.partial(dispatch_kernel, n_sp, n_tp),
        out_shape=(
            jax.ShapeDtypeStruct((slots, width_d), BF16),
            jax.ShapeDtypeStruct((slots, width_d), BF16),
            jax.ShapeDtypeStruct((n_sp * tokens, DV), BF16),
        ),
        in_specs=[vmem()] * 3,
        out_specs=(vmem(),) * 3,
        scratch_shapes=[
            dma((2,)), dma((2, n_sp)), dma((2,)), dma((2, n_sp, ones)),
            dma((2,)), dma((2,)), dma((1,)), dma((1,)),
        ],
        compiler_params=pltpu.CompilerParams(collective_id=0, has_side_effects=True),
        name="dispatch",
    )(routed, rows_in, mixer_out)

    w_gate, w_up, w_down = (weight_gate[0], weight_up[0], weight_down[0])
    gate_pre = jnp.dot(rows_in, w_gate, preferred_element_type=F32)
    up_pre = jnp.dot(rows_in, w_up, preferred_element_type=F32)
    sigmoid_g = jax.nn.sigmoid(gate_pre)
    active = gate_pre * sigmoid_g
    hidden = (active * up_pre).astype(BF16)
    across = (((1,), (1,)), ((), ()))
    back_grad = lax.dot_general(routed, w_down, across, preferred_element_type=F32)
    d_up = (back_grad * active).astype(BF16)
    d_gate = (back_grad * up_pre * sigmoid_g * (1.0 + gate_pre * (1.0 - sigmoid_g))).astype(BF16)
    grad_down = lax.dot_general(hidden, routed, contract, preferred_element_type=F32).astype(BF16)
    grad_gate = lax.dot_general(rows_in, d_gate, contract, preferred_element_type=F32).astype(BF16)
    grad_up = lax.dot_general(rows_in, d_up, contract, preferred_element_type=F32).astype(BF16)
    parts = lax.dot_general(d_gate, w_gate, across, preferred_element_type=F32)
    parts = parts + lax.dot_general(d_up, w_up, across, preferred_element_type=F32)
    parts = parts.astype(BF16)

    out_rows = width_d // n_sp
    proj, grad_q, grad_k, grad_v, grad_l = pl.pallas_call(
        functools.partial(return_kernel, n_sp, n_tp),
        out_shape=(
            jax.ShapeDtypeStruct((out_rows, DV), F32),
            jax.ShapeDtypeStruct((tokens, DK), BF16),
            jax.ShapeDtypeStruct((tokens, DK), BF16),
            jax.ShapeDtypeStruct((tokens, DV), BF16),
            jax.ShapeDtypeStruct((tokens, DK), F32),
        ),
        in_specs=[vmem()] * 9,
        out_specs=(vmem(),) * 5,
        scratch_shapes=[
            pltpu.VMEM((n_tp - 1, slots, width), BF16),
            pltpu.VMEM((slots, width), BF16),
            pltpu.VMEM((slots, width), BF16),
            pltpu.VMEM((tokens, width_d), BF16),
            pltpu.VMEM((width_d, tokens), BF16),
            pltpu.VMEM((n_sp, out_rows, tokens), BF16),
            pltpu.VMEM((DV, DK), BF16),
            pltpu.VMEM((n_sp, DV, DK), BF16),
            pltpu.VMEM((8, DK), F32),
            pltpu.VMEM((n_sp, 8, DK), F32),
            pltpu.VMEM((DV, DK), BF16),
            pltpu.VMEM((n_sp, DV, DK), BF16),
            pltpu.VMEM((DV, DK), F32),
            dma((1,)), dma((n_sp,)), dma((1,)), dma((1,)), dma((1,)), dma((1,)),
            dma((n_sp,)), dma((n_sp,)), dma((1,)), dma((1,)),
            dma((n_sp,)), dma((n_sp,)), dma((1,)), dma((1,)),
        ],
        compiler_params=pltpu.CompilerParams(collective_id=1, has_side_effects=True),
        name="combine",
    )(parts, picker, cotangent, out_weight, queries, key_vectors, values, log_decay, mixer_all)
    return (
        grad_gate[None], grad_up[None], grad_down[None], proj, grad_q, grad_k, grad_v, grad_l,
    )


def solution(mesh):
    n_sp, n_tp = mesh.shape["sp"], mesh.shape["tp"]
    return jax.shard_map(
        functools.partial(shards, n_sp, n_tp),
        mesh=mesh,
        in_specs=(
            P("sp", "tp"), P("sp", "tp"), P("sp", None), P("sp"), P("sp", None),
            P("sp", None, "tp"), P("sp", None, "tp"), P("sp", "tp", None), P(None, "tp"),
            P("sp", "tp"), P("sp", "tp"), P("sp", "tp"), P("sp", "tp"), P("sp", "tp"),
        ),
        out_specs=(
            P("sp", None, "tp"), P("sp", None, "tp"), P("sp", "tp", None),
            P("sp", "tp"), P("sp", "tp"), P("sp", "tp"), P("sp", "tp"), P("sp", "tp"),
        ),
        check_vma=False,
    )
```

time: 248 us -> 135 us (0.54)
  Pallas kernels: 0 us -> 107 us
  waiting for transfers between devices: 79.9 us -> 0 us
  blocking collectives: 56.5 us -> 0 us
  other arithmetic: 43.1 us -> 3.02 us
  between operations: 16.3 us -> 0.78 us
  local copies, waits for them, and re-layouts: 22 us -> 10.1 us
  matrix products: 23.4 us -> 13.6 us
  starting transfers between devices: 5.04 us -> 0 us
    pallas_call x0 -> x2, Pallas kernels: none -> 107 us  [the longest x1 65 us: shards(): pl.pallas_call(functools.partial(return_kernel, n_sp, n_tp), out_shape=(j...]
    all_gather x4 -> x0, waiting for transfers between devices: 43.1 us -> none  [the longest x1 29.8 us: shards(): lax.all_gather(routed, 'tp', axis=2, tiled=True)]
    all_to_all x2 -> x0, blocking collectives: 34.4 us -> none  [the longest x1 18.8 us: shards(): lax.all_to_all(rows_in, 'sp', split_axis=0, concat_axis=0, tiled=True)]
    reduce_scatter x2 -> x0, waiting for transfers between devices: 24.2 us -> none  [the longest x1 17.6 us: shards(): lax.psum_scatter(partial_rows.reshape(experts, capacity, width_d).astype(...]
    all_gather x2 -> x0, blocking collectives: 22.2 us -> none  [the longest x1 11.7 us: carried_in(): gathered = jax.tree.map(lambda a: lax.all_gather(a, axis), part)]
    all_to_all x1 -> x0, waiting for transfers between devices: 12.4 us -> none  [shards(): lax.all_to_all(summed, 'sp', split_axis=0, concat_axis=0, tiled=True)]
    dynamic_update_slice x14 -> x0, local copies, waits for them, and re-layouts: 11.6 us -> none  [local_forward(): lax.scan(block_step, state_in, (blocked(query_heads), blocked(key_heads),...]
    dot_general x29 -> x10, matrix products: 23.4 us -> 13.6 us  [the longest x1 2.09 us: shards(): gate_pre = jnp.dot(rows_in, w_gate, preferred_element_type=F32)]
  transfers between devices with their start and end apart: 7 -> 0, of which waited for: 5 -> 0; matrix products, arithmetic and copies ran while one was open for 31% -> 0% of each run, Pallas kernels for 0% -> 0%
where the time goes in v1:
time: 135 us
  Pallas kernels  107 us (79%)
  matrix products  13.6 us (10%)
  local copies, waits for them, and re-layouts  10.1 us (7%)
  other arithmetic  3.02 us (2%)
    pallas_call x1, Pallas kernels, shards(): pl.pallas_call(functools.partial(return_kernel, n_sp, n_tp), out_shape=(j...  65 us
    pallas_call x1, Pallas kernels, shards(): pl.pallas_call(functools.partial(dispatch_kernel, n_sp, n_tp), out_shape=...  42.2 us
    unnamed x16, local copies, waits for them, and re-layouts  9.14 us

profile of v1, /device:TPU:0, one launch (start us, length us, event | category | flops | bytes accessed | tf_op | source)
XLA Modules:
  0.0 134.6 jit_solution(6781316910562734703)
XLA Ops:
  0.6 0.8 copy.34
  1.6 0.6 reduce-window.6
  2.2 0.2 slice_reduce_fusion
  2.9 0.7 multiply_add_fusion
  3.8 0.7 broadcast_multiply_fusion
  4.9 2.0 %fusion.3.routed = bf16[384,512]{1,0:T(8,128)(2,1)} fusion(pred[128,384]{1,0:T(8,128)(4,1)S(1)} %fusion.13, bf16[128,512]{1,0:T(8,128)(2,1)} %cotangent.1, f32[384]{0:T(512)S(1)} %select_reduce_fusion), kind=kOutput, calls=%fused_computation.8 | convolution fusion | flops 50724864 | bytes 574976 | tf_op jit(solution)/shard_map/dot_general | solution.py:409
  6.8 2.0 %convolution_convert_fusion.3.rows_in = bf16[384,512]{1,0:T(8,128)(2,1)} fusion(pred[128,384]{1,0:T(8,128)(4,1)S(1)} %fusion.13, bf16[128,512]{1,0:T(8,128)(2,1)} %param.15), kind=kOutput, calls=%fused_computation.9 | convolution fusion | flops 50528256 | bytes 573440 | tf_op jit(solution)/shard_map/dot_general | solution.py:410
  8.8 42.2 %dispatch.1 = (bf16[384,2048]{1,0:T(8,128)(2,1)}, bf16[384,2048]{1,0:T(8,128)(2,1)}, bf16[1024,256]{1,0:T(8,128)(2,1)}) custom-call(bf16[384,512]{1,0:T(8,128)(2,1)} %fusion.3.routed, bf16[384,512]{1,0:T(8,128)(2,1)} %convolution_convert_fusion.3.rows_in, bf16[128,256]{1,0:T(8,128)(2,1)} %mixer.1), custom_call_target="tpu_custom_call" | custom-call | tf_op jit(solution)/shard_map/dispatch/pallas_call | solution.py:415
  51.0 2.1 %fusion.6 = f32[384,128]{1,0:T(8,128)S(1)} fusion(bf16[384,2048]{1,0:T(8,128)(2,1)} %get-tuple-element.16, bf16[1,2048,128]{2,1,0:T(8,128)(2,1)S(1)} %copy-done), kind=kOutput, calls=%fused_computation.12 | convolution fusion | flops 201326592 | bytes 2293760 | tf_op jit(solution)/shard_map/dot_general | solution.py:433
  53.1 0.6 fusion.9
  53.7 0.8 copy-done.3
  54.6 0.6 multiply_convert_fusion.1
  55.2 1.4 %fusion = bf16[1,2048,128]{2,1,0:T(8,128)(2,1)} fusion(bf16[384,2048]{1,0:T(8,128)(2,1)S(1)} %copy-done.1, bf16[384,128]{1,0:T(8,128)(2,1)S(1)} %get-tuple-element.25), kind=kOutput, calls=%fused_computation.4 | convolution fusion | flops 201588736 | bytes 2195456 | tf_op jit(solution)/shard_map/dot_general | solution.py:443
  56.6 1.4 %fusion.1 = bf16[1,2048,128]{2,1,0:T(8,128)(2,1)} fusion(bf16[384,2048]{1,0:T(8,128)(2,1)S(1)} %copy-done.1, bf16[384,128]{1,0:T(8,128)(2,1)S(1)} %get-tuple-element.24), kind=kOutput, calls=%fused_computation.5 | convolution fusion | flops 201588736 | bytes 2195456 | tf_op jit(solution)/shard_map/dot_general | solution.py:444
  58.0 1.3 fusion.2
  59.3 0.6 fusion.4
  59.9 1.7 %add_convert_fusion.parts = bf16[384,2048]{1,0:T(8,128)(2,1)} fusion(f32[384,2048]{1,0:T(8,128)S(1)} %fusion.4, bf16[384,128]{1,0:T(8,128)(2,1)S(1)} %get-tuple-element.24, bf16[1,2048,128]{2,1,0:T(8,128)(2,1)S(1)} %copy-done.2), kind=kOutput, calls=%fused_computation | convolution fusion | flops 202899456 | bytes 5341184 | tf_op jit(solution)/shard_map/dot_general | solution.py:446
  61.6 0.7 convert_element_type.48.picker
  62.3 65.0 %combine.1 = (f32[256,256]{1,0:T(8,128)}, bf16[128,128]{1,0:T(8,128)(2,1)}, bf16[128,128]{1,0:T(8,128)(2,1)}, bf16[128,256]{1,0:T(8,128)(2,1)}, f32[128,128]{1,0:T(8,128)}) custom-call(bf16[384,2048]{1,0:T(8,128)(2,1)} %add_convert_fusion.parts, bf16[128,384]{1,0:T(8,128)(2,1)} %convert_element_type.48.picker, bf16[128,512]{1,0:T(8,128)(2,1)} %cotangent.1, ...), custom_call_target="tpu_custom_call" | custom-call | tf_op jit(solution)/shard_map/combine/pallas_call | solution.py:450
  127.3 1.7 %copy.43 = f32[256,256]{1,0:T(8,128)} copy(f32[256,256]{1,0:T(8,128)} %get-tuple-element.37) | data formatting | bytes 524288
  128.9 1.4 %copy.44 = bf16[128,128]{1,0:T(8,128)(2,1)} copy(bf16[128,128]{1,0:T(8,128)(2,1)} %get-tuple-element.38) | data formatting | bytes 65536
  130.3 1.4 %copy.45 = bf16[128,128]{1,0:T(8,128)(2,1)} copy(bf16[128,128]{1,0:T(8,128)(2,1)} %get-tuple-element.39) | data formatting | bytes 65536
  131.7 1.5 %copy.46 = bf16[128,256]{1,0:T(8,128)(2,1)} copy(bf16[128,256]{1,0:T(8,128)(2,1)} %get-tuple-element.40) | data formatting | bytes 131072
  133.2 1.5 %copy.47 = f32[128,128]{1,0:T(8,128)} copy(f32[128,128]{1,0:T(8,128)} %get-tuple-element.41) | data formatting | bytes 131072
  (22 shorter events, 1.3 us)
Async XLA Ops:
  0.6 50.4 %copy-start = (bf16[1,2048,128]{2,1,0:T(8,128)(2,1)S(1)}, bf16[1,2048,128]{2,1,0:T(8,128)(2,1)}, u32[]{:S(2)}) copy-start(bf16[1,2048,128]{2,1,0:T(8,128)(2,1)} %param.19) | copy-start | bytes 1572868
  8.8 44.3 %copy-start.2 = (bf16[1,2048,128]{2,1,0:T(8,128)(2,1)S(1)}, bf16[1,2048,128]{2,1,0:T(8,128)(2,1)}, u32[]{:S(2)}) copy-start(bf16[1,2048,128]{2,1,0:T(8,128)(2,1)} %param.20) | copy-start | bytes 1572868
  51.0 2.1 %copy-start.1 = (bf16[384,2048]{1,0:T(8,128)(2,1)S(1)}, bf16[384,2048]{1,0:T(8,128)(2,1)}, u32[]{:S(2)}) copy-start(bf16[384,2048]{1,0:T(8,128)(2,1)} %get-tuple-element.16) | copy-start | bytes 4718596
  53.1 1.4 %copy-start.3 = (bf16[384,2048]{1,0:T(8,128)(2,1)S(1)}, bf16[384,2048]{1,0:T(8,128)(2,1)}, u32[]{:S(2)}) copy-start(bf16[384,2048]{1,0:T(8,128)(2,1)} %get-tuple-element.17) | copy-start | bytes 4718596
  53.1 1.5 %copy-start.4 = (bf16[1,128,2048]{2,1,0:T(8,128)(2,1)S(1)}, bf16[1,128,2048]{2,1,0:T(8,128)(2,1)}, u32[]{:S(2)}) copy-start(bf16[1,128,2048]{2,1,0:T(8,128)(2,1)} %param.21) | copy-start | bytes 1572868

commit v2 on v1

--- a/solution.py
+++ b/solution.py
@@ -26,8 +26,6 @@
 
 
 def sp_order(n_sp):
-    if n_sp % 2:
-        return [(d, 0) for d in range(1, n_sp)], n_sp, 1
     z = n_sp // 2
     places = [(dz, dc) for dz in range(z) for dc in range(2)][1:]
     places.sort(key=lambda p: (min(p[0], z - p[0]), p))
@@ -40,6 +38,8 @@
         self.sp, self.tp = lax.axis_index("sp"), lax.axis_index("tp")
         self.order, self.z, self.cores = sp_order(n_sp)
         self.rows, self.cols = tp_grid(n_tp)
+        self.chip, self.core = self.sp // self.cores, self.sp % self.cores
+        self.chips = sorted(range(1, self.z), key=lambda dz: (min(dz, self.z - dz), dz))
 
     def sp_peer(self, place, back=False):
         dz, dc = place
@@ -72,7 +72,7 @@
     pltpu.make_async_copy(ref, ref, sem).wait()
 
 
-def meet(here):
+def greet(here):
     barrier = pltpu.get_barrier_semaphore()
     for place in here.order:
         pl.semaphore_signal(
@@ -82,7 +82,19 @@
         pl.semaphore_signal(
             barrier, inc=1, device_id=(here.sp, here.tp_peer(off)), device_id_type=MESH
         )
-    pl.semaphore_wait(barrier, here.n_sp + here.n_tp - 2)
+
+
+def greeted(here):
+    pl.semaphore_wait(pltpu.get_barrier_semaphore(), here.n_sp + here.n_tp - 2)
+
+
+def meet(here):
+    greet(here)
+    greeted(here)
+
+
+def pull(picker, rows):
+    return lax.dot_general(picker, rows, (((0,), (0,)), ((), ())), preferred_element_type=F32)
 
 
 def at(start, size):
@@ -90,17 +102,23 @@
 
 
 def dispatch_kernel(
-    n_sp, n_tp, routed, rows_in, mixer, out_routed, out_rows, mixer_all,
+    n_sp, n_tp, picker, weight, cotangent, moe_input, mixer, out_routed, out_rows, mixer_all,
+    routed, rows_in,
     sp_send, sp_recv, one_send, one_recv, two_send, two_recv, mix_send, mix_recv,
+    pair_send, pair_recv,
 ):
     here = Place(n_sp, n_tp)
     cap, width = routed.shape[0] // n_sp, routed.shape[1]
     tok = mixer.shape[0]
-    meet(here)
+    greet(here)
+    chosen = picker[...]
+    routed[...] = (weight[...] * pull(chosen, cotangent[...])).astype(BF16)
+    rows_in[...] = pull(chosen, moe_input[...]).astype(BF16)
+    greeted(here)
     pairs = ((0, routed, out_routed), (1, rows_in, out_rows))
-    for a, src, dst in pairs:
-        for k, place in enumerate(here.order):
-            peer = here.sp_peer(place)
+    for k, place in enumerate(here.order):
+        peer = here.sp_peer(place)
+        for a, src, dst in pairs:
             send(
                 src.at[at(peer, cap)], dst.at[at(here.sp, cap), at(here.tp, width)],
                 sp_send.at[a], sp_recv.at[a, k], peer, here.tp,
@@ -135,10 +153,12 @@
     last = len(here.order)
     for a, src, dst in pairs:
         spread(a, last, here.sp, src.at[at(here.sp, cap)], dst)
-    for place in here.order:
+    mate = here.sp_peer((0, 1))
+    mine = mixer_all.at[at(here.sp, tok)]
+    send(mixer, mine, pair_send.at[0], pair_recv.at[0], mate, here.tp)
+    for dz in here.chips:
         send(
-            mixer, mixer_all.at[at(here.sp, tok)], mix_send.at[0], mix_recv.at[0],
-            here.sp_peer(place), here.tp,
+            mixer, mine, mix_send.at[0], mix_recv.at[dz], here.sp_peer((dz, 0)), here.tp
         )
     for a, src, dst in pairs:
         dst[at(here.sp, cap), at(here.tp, width)] = src[at(here.sp, cap), :]
@@ -154,6 +174,10 @@
                 spread(a, k_next, sources[k_next], block, dst)
         for a, src, dst in pairs:
             relay(a, k, sources[k], dst)
+    for dz in here.chips:
+        block = mixer_all.at[at(here.sp_peer((dz, 0), back=True), tok)]
+        wait_bytes(block, mix_recv.at[dz])
+        send(block, block, pair_send.at[0], pair_recv.at[0], mate, here.tp)
     for a, src, dst in pairs:
         count = here.cols - 1 if a == 0 else here.rows - 1
         twos = (here.rows - 1 if a == 0 else here.cols - 1) * (1 + count)
@@ -161,8 +185,9 @@
         wait_bytes(dst.at[:, pl.ds(0, twos * width)], two_send.at[a])
         wait_bytes(dst.at[:, pl.ds(0, count * width)], one_send.at[a])
         wait_bytes(src.at[pl.ds(0, (n_sp - 1) * cap)], sp_send.at[a])
-    wait_bytes(mixer_all.at[pl.ds(0, (n_sp - 1) * tok)], mix_recv.at[0])
-    wait_bytes(mixer_all.at[pl.ds(0, (n_sp - 1) * tok)], mix_send.at[0])
+    wait_bytes(mixer_all.at[pl.ds(0, (here.z - 1) * tok)], mix_send.at[0])
+    wait_bytes(mixer_all.at[pl.ds(0, here.z * tok)], pair_recv.at[0])
+    wait_bytes(mixer_all.at[pl.ds(0, here.z * tok)], pair_send.at[0])
 
 
 def mm(a, b, ca, cb, precision=HIGHEST):
@@ -180,10 +205,10 @@
 def return_kernel(
     n_sp, n_tp, parts, picker, cotangent, out_weight, queries, keys, values, decay, mixer_all,
     proj, grad_q, grad_k, grad_v, grad_l,
-    got, summed, returned, piece, piece_t, pieces, carry, carries, total, totals, back, backs,
-    state,
-    tp_send, tp_recv, sp_send, sp_recv, piece_send, piece_recv, carry_send, carry_recv,
-    total_send, total_recv, back_send, back_recv, res_send, res_recv,
+    got, summed, returned, piece, piece_t, pieces, own, other, half, halves, total, totals,
+    state, edges,
+    tp_send, tp_recv, sp_send, sp_recv, piece_send, piece_recv, mate_send, mate_recv,
+    half_send, half_recv, edge_send, edge_recv, total_send, total_recv, res_send, res_recv,
 ):
     here = Place(n_sp, n_tp)
     me = here.sp
@@ -222,18 +247,73 @@
         key_end = keys[rows, :].astype(F32) * jnp.exp(ends[b] - cums[b])
         fresh = mm(values[rows, :].astype(F32), key_end, 0, 0)
         term = fresh if term is None else jnp.exp(ends[b]) * term + fresh
-    carry[...] = term.astype(BF16)
+    own[0] = term.astype(BF16)
     total[...] = jnp.broadcast_to(span, total.shape)
-    for k, place in enumerate(here.order):
-        peer = here.sp_peer(place)
+    mate = here.sp_peer((0, 1))
+    first_core = here.core == 0
+    rows_half = half.shape[1]
+    send(own.at[0], other.at[0], mate_send.at[0], mate_recv.at[0], mate, here.tp)
+    for place in here.order:
         send(
-            total, totals.at[me], total_send.at[0], total_recv.at[0], peer, here.tp
-        )
-
-        @pl.when(peer > me)
-        def _():
-            send(carry, carries.at[me], carry_send.at[k], carry_recv.at[k], peer, here.tp)
-
+            total, totals.at[me], total_send.at[0], total_recv.at[0],
+            here.sp_peer(place), here.tp,
+        )
+
+    def in_order(way):
+        mine, theirs = own[way].astype(F32), other[way].astype(F32)
+        return jnp.where(first_core, mine, theirs), jnp.where(first_core, theirs, mine)
+
+    def share(way):
+        wait_bytes(other.at[way], mate_recv.at[way])
+        early, late = in_order(way)
+        here_early = jnp.exp(totals[here.chip * 2, 0:1, :])
+        here_late = jnp.exp(totals[here.chip * 2 + 1, 0:1, :])
+        chip = (here_late * early + late) if way == 0 else (early + here_early * late)
+        half[way] = jnp.where(first_core, chip[:rows_half], chip[rows_half:]).astype(BF16)
+        for dz in here.chips:
+            far = (here.chip + dz) % here.z
+            needed = (far > here.chip) if way == 0 else (far < here.chip)
+
+            @pl.when(needed)
+            def _():
+                send(
+                    half.at[way], halves.at[way, here.chip], half_send.at[way, dz],
+                    half_recv.at[way, dz], here.sp_peer((dz, 0)), here.tp,
+                )
+
+    def settle(way):
+        for dz in here.chips:
+            far = (here.chip + here.z - dz) % here.z
+            needed = (far < here.chip) if way == 0 else (far > here.chip)
+
+            @pl.when(needed)
+            def _():
+                wait_bytes(half.at[way], half_recv.at[way, dz])
+
+        state[...] = jnp.zeros_like(state)
+        for z in range(here.z) if way == 0 else reversed(range(here.z)):
+            @pl.when((z < here.chip) if way == 0 else (z > here.chip))
+            def _():
+                decays = jnp.exp(totals[2 * z, 0:1, :] + totals[2 * z + 1, 0:1, :])
+                state[...] = decays * state[...] + halves[way, z].astype(F32)
+
+        edges[way, here.core] = state[...]
+        send(
+            edges.at[way, here.core], edges.at[way, here.core],
+            edge_send.at[way], edge_recv.at[way], mate, here.tp,
+        )
+        wait_bytes(state, edge_recv.at[way])
+        chip_edge = jnp.concatenate([edges[way, 0], edges[way, 1]], axis=0)
+        early, late = in_order(way)
+        if way == 0:
+            passed = jnp.exp(totals[here.chip * 2, 0:1, :]) * chip_edge + early
+            return jnp.where(first_core, chip_edge, passed)
+        passed = jnp.exp(totals[here.chip * 2 + 1, 0:1, :]) * chip_edge + late
+        return jnp.where(first_core, passed, chip_edge)
+
+    wait_bytes(totals.at[pl.ds(0, n_sp - 1)], total_recv.at[0])
+    totals[me] = total[...]
+    share(0)
     for k, place in enumerate(order + [None]):
         source = me if place is None else here.sp_peer(place)
         wait_bytes(got.at[:, at(source, cap)], tp_recv.at[k])
@@ -258,22 +338,7 @@
             piece_send.at[0], piece_recv.at[0], me, here.tp_peer(off),
         )
 
-    wait_bytes(totals.at[pl.ds(0, n_sp - 1)], total_recv.at[0])
-    totals[me] = total[...]
-    for k, place in enumerate(here.order):
-        source = here.sp_peer(place, back=True)
-
-        @pl.when(source < me)
-        def _():
-            wait_bytes(carry, carry_recv.at[k])
-
-    state[...] = jnp.zeros_like(state)
-    for s in range(n_sp):
-        @pl.when(s < me)
-        def _():
-            state[...] = jnp.exp(totals[s, 0:1, :]) * state[...] + carries[s].astype(F32)
-
-    states = [state[...]]
+    states = [settle(0)]
     for b in range(blocks):
         rows = slice(b * BLK, (b + 1) * BLK)
         key_end = keys[rows, :].astype(F32) * jnp.exp(ends[b] - cums[b])
@@ -290,14 +355,9 @@
         query_dec = queries[rows, :].astype(F32) * (scale * jnp.exp(cums[b]))
         fresh = mm(mix[rows, :], query_dec, 0, 0)
         term = fresh if term is None else jnp.exp(ends[b]) * term + fresh
-    back[...] = term.astype(BF16)
-    for k, place in enumerate(here.order):
-        peer = here.sp_peer(place)
-
-        @pl.when(peer < me)
-        def _():
-            send(back, backs.at[me], back_send.at[k], back_recv.at[k], peer, here.tp)
-
+    own[1] = term.astype(BF16)
+    send(own.at[1], other.at[1], mate_send.at[1], mate_recv.at[1], mate, here.tp)
+    share(1)
     piece_t[...] = whole.T
     for place in here.order:
         peer = here.sp_peer(place)
@@ -321,20 +381,7 @@
         grad_q[rows, :] = d_query.astype(BF16)
         kept.append((d_query, d_key, d_value))
 
-    for k, place in enumerate(here.order):
-        source = here.sp_peer(place, back=True)
-
-        @pl.when(source > me)
-        def _():
-            wait_bytes(back, back_recv.at[k])
-
-    state[...] = jnp.zeros_like(state)
-    for s in reversed(range(n_sp)):
-        @pl.when(s > me)
-        def _():
-            state[...] = jnp.exp(totals[s, 0:1, :]) * state[...] + backs[s].astype(F32)
-
-    leaving = state[...]
+    leaving = settle(1)
     edge = jnp.sum(states[blocks] * leaving, axis=0, keepdims=True)
     terms = [None] * blocks
     for b in reversed(range(blocks)):
@@ -370,16 +417,21 @@
     wait_bytes(piece.at[:, pl.ds(0, (n_tp - 1) * width)], piece_send.at[0])
     wait_bytes(totals.at[pl.ds(0, n_sp - 1)], total_send.at[0])
     wait_bytes(pieces.at[pl.ds(0, n_sp - 1)], res_send.at[0])
-    for k, place in enumerate(here.order):
-        peer = here.sp_peer(place)
-
-        @pl.when(peer > me)
-        def _():
-            wait_bytes(carry, carry_send.at[k])
-
-        @pl.when(peer < me)
-        def _():
-            wait_bytes(back, back_send.at[k])
+    for way in range(2):
+        wait_bytes(own.at[way], mate_send.at[way])
+        wait_bytes(state, edge_send.at[way])
+        for dz in here.chips:
+            far = (here.chip + dz) % here.z
+
+            @pl.when((far > here.chip) if way == 0 else (far < here.chip))
+            def _():
+                wait_bytes(half.at[way], half_send.at[way, dz])
+
+
+def finish_kernel(*refs):
+    count = len(refs) // 2
+    for source, target in zip(refs[:count], refs[count:]):
+        target[...] = source[...]
 
 
 def vmem():
@@ -406,9 +458,6 @@
     slot_weight = jnp.sum(jnp.where(slot_match, route_weight[:, None], 0.0), axis=0)
     picker = jnp.any(slot_match.reshape(tokens, 2, -1), axis=1).astype(BF16)
     contract = (((0,), (0,)), ((), ()))
-    pulled_grad = lax.dot_general(picker, cotangent, contract, preferred_element_type=F32)
-    rows_in = lax.dot_general(picker, moe_input, contract, preferred_element_type=F32).astype(BF16)
-    routed = (slot_weight[:, None] * pulled_grad).astype(BF16)
 
     dma, rows_tp, cols_tp = pltpu.SemaphoreType.DMA, *tp_grid(n_tp)
     ones = max(rows_tp, cols_tp) - 1
@@ -419,15 +468,17 @@
             jax.ShapeDtypeStruct((slots, width_d), BF16),
             jax.ShapeDtypeStruct((n_sp * tokens, DV), BF16),
         ),
-        in_specs=[vmem()] * 3,
+        in_specs=[vmem()] * 5,
         out_specs=(vmem(),) * 3,
         scratch_shapes=[
+            pltpu.VMEM((slots, width), BF16), pltpu.VMEM((slots, width), BF16),
             dma((2,)), dma((2, n_sp)), dma((2,)), dma((2, n_sp, ones)),
-            dma((2,)), dma((2,)), dma((1,)), dma((1,)),
+            dma((2,)), dma((2,)), dma((1,)), dma((n_sp,)),
+            dma((1,)), dma((1,)),
         ],
         compiler_params=pltpu.CompilerParams(collective_id=0, has_side_effects=True),
         name="dispatch",
-    )(routed, rows_in, mixer_out)
+    )(picker, slot_weight[:, None], cotangent, moe_input, mixer_out)
 
     w_gate, w_up, w_down = (weight_gate[0], weight_up[0], weight_down[0])
     gate_pre = jnp.dot(rows_in, w_gate, preferred_element_type=F32)
@@ -447,15 +498,16 @@
     parts = parts.astype(BF16)
 
     out_rows = width_d // n_sp
-    proj, grad_q, grad_k, grad_v, grad_l = pl.pallas_call(
+    shapes = (
+        jax.ShapeDtypeStruct((out_rows, DV), F32),
+        jax.ShapeDtypeStruct((tokens, DK), BF16),
+        jax.ShapeDtypeStruct((tokens, DK), BF16),
+        jax.ShapeDtypeStruct((tokens, DV), BF16),
+        jax.ShapeDtypeStruct((tokens, DK), F32),
+    )
+    results = pl.pallas_call(
         functools.partial(return_kernel, n_sp, n_tp),
-        out_shape=(
-            jax.ShapeDtypeStruct((out_rows, DV), F32),
-            jax.ShapeDtypeStruct((tokens, DK), BF16),
-            jax.ShapeDtypeStruct((tokens, DK), BF16),
-            jax.ShapeDtypeStruct((tokens, DV), BF16),
-            jax.ShapeDtypeStruct((tokens, DK), F32),
-        ),
+        out_shape=shapes,
         in_specs=[vmem()] * 9,
         out_specs=(vmem(),) * 5,
         scratch_shapes=[
@@ -465,20 +517,25 @@
             pltpu.VMEM((tokens, width_d), BF16),
             pltpu.VMEM((width_d, tokens), BF16),
             pltpu.VMEM((n_sp, out_rows, tokens), BF16),
-            pltpu.VMEM((DV, DK), BF16),
-            pltpu.VMEM((n_sp, DV, DK), BF16),
+            pltpu.VMEM((2, DV, DK), BF16),
+            pltpu.VMEM((2, DV, DK), BF16),
+            pltpu.VMEM((2, DV // 2, DK), BF16),
+            pltpu.VMEM((2, n_sp // 2, DV // 2, DK), BF16),
             pltpu.VMEM((8, DK), F32),
             pltpu.VMEM((n_sp, 8, DK), F32),
-            pltpu.VMEM((DV, DK), BF16),
-            pltpu.VMEM((n_sp, DV, DK), BF16),
-            pltpu.VMEM((DV, DK), F32),
+            pltpu.VMEM((DV // 2, DK), F32),
+            pltpu.VMEM((2, 2, DV // 2, DK), F32),
             dma((1,)), dma((n_sp,)), dma((1,)), dma((1,)), dma((1,)), dma((1,)),
-            dma((n_sp,)), dma((n_sp,)), dma((1,)), dma((1,)),
-            dma((n_sp,)), dma((n_sp,)), dma((1,)), dma((1,)),
+            dma((2,)), dma((2,)), dma((2, n_sp // 2)), dma((2, n_sp // 2)),
+            dma((2,)), dma((2,)), dma((1,)), dma((1,)), dma((1,)), dma((1,)),
         ],
         compiler_params=pltpu.CompilerParams(collective_id=1, has_side_effects=True),
         name="combine",
     )(parts, picker, cotangent, out_weight, queries, key_vectors, values, log_decay, mixer_all)
+    proj, grad_q, grad_k, grad_v, grad_l = pl.pallas_call(
+        finish_kernel, out_shape=shapes, in_specs=[vmem()] * 5, out_specs=(vmem(),) * 5,
+        name="finish",
+    )(*results)
     return (
         grad_gate[None], grad_up[None], grad_down[None], proj, grad_q, grad_k, grad_v, grad_l,
     )

time: 135 us -> 107 us (0.79)
  Pallas kernels: 107 us -> 90 us
  local copies, waits for them, and re-layouts: 10.1 us -> 3.46 us
  matrix products: 13.6 us -> 9.67 us
    pallas_call x1 -> x2, Pallas kernels: 65 us -> 51.7 us  [the longest x1 50 us: shards(): pl.pallas_call(functools.partial(return_kernel, n_sp, n_tp), out_shape=sh...]
    unnamed x16 -> x11, local copies, waits for them, and re-layouts: 9.14 us -> 1.73 us
    dot_general x2 -> x0, matrix products: 3.93 us -> none  [the longest x1 1.97 us: shards(): lax.dot_general(picker, cotangent, contract, preferred_element_type=F32)]
    pallas_call x1, Pallas kernels: 42.2 us -> 38.3 us  [shards(): pl.pallas_call(functools.partial(dispatch_kernel, n_sp, n_tp), out_shape=...]
where the time goes in v2:
time: 107 us
  Pallas kernels  90 us (84%)
  matrix products  9.67 us (9%)
  local copies, waits for them, and re-layouts  3.46 us (3%)
  other arithmetic  3.07 us (3%)
    pallas_call x1, Pallas kernels, shards(): pl.pallas_call(functools.partial(return_kernel, n_sp, n_tp), out_shape=sh...  50 us
    pallas_call x1, Pallas kernels, shards(): pl.pallas_call(functools.partial(dispatch_kernel, n_sp, n_tp), out_shape=...  38.3 us

profile of v2, /device:TPU:0, one launch (start us, length us, event | category | flops | bytes accessed | tf_op | source)
XLA Modules:
  0.0 107.0 jit_solution(17981243422237001432)
XLA Ops:
  0.6 0.7 broadcast_multiply_fusion
  1.5 0.1 broadcast_in_dim.30
  1.6 0.8 copy.36
  2.4 0.1 eq.45
  2.6 0.1 eq.49
  2.7 0.6 reduce-window.6
  3.3 0.2 slice_reduce_fusion
  3.7 0.2 select_reduce_fusion
  3.8 0.1 reduce_sum.21
  4.0 0.7 multiply_add_fusion.1
  4.9 0.6 convert_element_type.33.picker
  5.5 0.8 broadcast_in_dim.37.weight
  6.3 38.3 %dispatch.1 = (bf16[384,2048]{1,0:T(8,128)(2,1)}, bf16[384,2048]{1,0:T(8,128)(2,1)}, bf16[1024,256]{1,0:T(8,128)(2,1)}) custom-call(bf16[128,384]{1,0:T(8,128)(2,1)} %convert_element_type.33.picker, f32[384,1]{1,0:T(8,128)} %broadcast_in_dim.37.weight, bf16[128,512]{1,0:T(8,128)(2,1)} %cotangent.3, bf16[128,512]{1,0:T(8,128)(2,1)} %moe_input.1, ...), custom_call_target="tpu_custom_call" | custom-call | tf_op jit(solution)/shard_map/dispatch/pallas_call | solution.py:464
  44.6 2.1 %fusion.5 = f32[384,128]{1,0:T(8,128)S(1)} fusion(bf16[384,2048]{1,0:T(8,128)(2,1)} %get-tuple-element.21, bf16[1,2048,128]{2,1,0:T(8,128)(2,1)S(1)} %copy-done), kind=kOutput, calls=%fused_computation.9 | convolution fusion | flops 201326592 | bytes 2293760 | tf_op jit(solution)/shard_map/dot_general | solution.py:484
  46.8 0.6 fusion.8
  47.3 0.8 copy-done.3
  48.2 0.6 multiply_convert_fusion.1
  48.8 1.3 %fusion.2 = bf16[1,128,2048]{2,1,0:T(8,128)(2,1)} fusion(bf16[384,2048]{1,0:T(8,128)(2,1)S(1)} %copy-done.3, f32[384,128]{1,0:T(8,128)S(1)} %fusion.8, f32[384,128]{1,0:T(8,128)S(1)} %fusion.5), kind=kOutput, calls=%fused_computation.6 | convolution fusion | flops 201883648 | bytes 2490368 | tf_op jit(solution)/shard_map/dot_general | solution.py:493
  50.1 1.4 %fusion.1 = bf16[1,2048,128]{2,1,0:T(8,128)(2,1)} fusion(bf16[384,2048]{1,0:T(8,128)(2,1)S(1)} %copy-done.1, bf16[384,128]{1,0:T(8,128)(2,1)S(1)} %get-tuple-element.34), kind=kOutput, calls=%fused_computation.5 | convolution fusion | flops 201588736 | bytes 2195456 | tf_op jit(solution)/shard_map/dot_general | solution.py:495
  51.5 1.4 %fusion = bf16[1,2048,128]{2,1,0:T(8,128)(2,1)} fusion(bf16[384,2048]{1,0:T(8,128)(2,1)S(1)} %copy-done.1, bf16[384,128]{1,0:T(8,128)(2,1)S(1)} %get-tuple-element.35), kind=kOutput, calls=%fused_computation.4 | convolution fusion | flops 201588736 | bytes 2195456 | tf_op jit(solution)/shard_map/dot_general | solution.py:494
  53.0 0.6 fusion.3
  53.5 1.7 %add_convert_fusion.parts = bf16[384,2048]{1,0:T(8,128)(2,1)} fusion(f32[384,2048]{1,0:T(8,128)S(1)} %fusion.3, bf16[384,128]{1,0:T(8,128)(2,1)S(1)} %get-tuple-element.34, bf16[1,2048,128]{2,1,0:T(8,128)(2,1)S(1)} %copy-done.2), kind=kOutput, calls=%fused_computation | convolution fusion | flops 202899456 | bytes 5341184 | tf_op jit(solution)/shard_map/dot_general | solution.py:497
  55.3 50.0 %combine.1 = (f32[256,256]{1,0:T(8,128)}, bf16[128,128]{1,0:T(8,128)(2,1)}, bf16[128,128]{1,0:T(8,128)(2,1)}, bf16[128,256]{1,0:T(8,128)(2,1)}, f32[128,128]{1,0:T(8,128)}) custom-call(bf16[384,2048]{1,0:T(8,128)(2,1)} %add_convert_fusion.parts, bf16[128,384]{1,0:T(8,128)(2,1)} %convert_element_type.33.picker, bf16[128,512]{1,0:T(8,128)(2,1)} %cotangent.3, ...), custom_call_target="tpu_custom_call" | custom-call | tf_op jit(solution)/shard_map/combine/pallas_call | solution.py:508
  105.2 1.8 %finish.1 = (f32[256,256]{1,0:T(8,128)}, bf16[128,128]{1,0:T(8,128)(2,1)}, bf16[128,128]{1,0:T(8,128)(2,1)}, bf16[128,256]{1,0:T(8,128)(2,1)}, f32[128,128]{1,0:T(8,128)}) custom-call(f32[256,256]{1,0:T(8,128)} %get-tuple-element.24.refs_0_, bf16[128,128]{1,0:T(8,128)(2,1)} %get-tuple-element.25.refs_1_, bf16[128,128]{1,0:T(8,128)(2,1)} %get-tuple-element.26.refs_2_, ...), custom_call_target="tpu_custom_call" | custom-call | tf_op jit(solution)/shard_map/finish/pallas_call | solution.py:535
  (17 shorter events, 0.6 us)
Async XLA Ops:
  0.6 44.0 %copy-start = (bf16[1,2048,128]{2,1,0:T(8,128)(2,1)S(1)}, bf16[1,2048,128]{2,1,0:T(8,128)(2,1)}, u32[]{:S(2)}) copy-start(bf16[1,2048,128]{2,1,0:T(8,128)(2,1)} %param.19) | copy-start | bytes 1572868
  5.5 41.2 %copy-start.2 = (bf16[1,2048,128]{2,1,0:T(8,128)(2,1)S(1)}, bf16[1,2048,128]{2,1,0:T(8,128)(2,1)}, u32[]{:S(2)}) copy-start(bf16[1,2048,128]{2,1,0:T(8,128)(2,1)} %param.20) | copy-start | bytes 1572868
  44.6 2.1 %copy-start.1 = (bf16[384,2048]{1,0:T(8,128)(2,1)S(1)}, bf16[384,2048]{1,0:T(8,128)(2,1)}, u32[]{:S(2)}) copy-start(bf16[384,2048]{1,0:T(8,128)(2,1)} %get-tuple-element.21) | copy-start | bytes 4718596
  46.7 1.4 %copy-start.3 = (bf16[384,2048]{1,0:T(8,128)(2,1)S(1)}, bf16[384,2048]{1,0:T(8,128)(2,1)}, u32[]{:S(2)}) copy-start(bf16[384,2048]{1,0:T(8,128)(2,1)} %get-tuple-element.22) | copy-start | bytes 4718596
  46.7 1.5 %copy-start.4 = (bf16[1,128,2048]{2,1,0:T(8,128)(2,1)S(1)}, bf16[1,128,2048]{2,1,0:T(8,128)(2,1)}, u32[]{:S(2)}) copy-start(bf16[1,128,2048]{2,1,0:T(8,128)(2,1)} %param.21) | copy-start | bytes 1572868
